TPU v7x, 768 devices: a whole 4x8x12 slice. The times are simulated.
768 devices in a mesh: sp: 48 (over z, x), tp: 16 (over y, core).
Axes of the slice: x: 4, y: 8, z: 12, core: 2. Of those that a mesh axis runs over, the one named last changes fastest.
Arguments:
- tokens: bfloat16 [48, 480, 4096], P(None, 'sp', 'tp'), may hold values from -6 to 6
- latent_down_weight: bfloat16 [4096, 512], replicated, may hold values from -0.09375 to 0.09375
- w_rope_key: bfloat16 [4096, 64], replicated, may hold values from -0.09375 to 0.09375
- latent_norm_gain: float32 [512], replicated, may hold values from 0.1 to 1.9
- key_up_weight: bfloat16 [512, 4096], P(None, 'tp'), may hold values from -0.25 to 0.25
- value_up_weight: bfloat16 [512, 4096], P(None, 'tp'), may hold values from -0.25 to 0.25
- cached_latent_rows: bfloat16 [48, 32768, 512], P('sp', 'tp'), may hold values from -6 to 6
- past_rope: bfloat16 [48, 32768, 64], P('sp', 'tp'), may hold values from -6 to 6
- query_nope: bfloat16 [48, 4096], P('sp', 'tp'), may hold values from -8 to 8
- query_rope: bfloat16 [48, 2048], P('sp', 'tp'), may hold values from -300 to 300
Outputs:
- new_keys: bfloat16 [48, 480, 4096], P('sp', None, 'tp')
- new_values: bfloat16 [48, 480, 4096], P('sp', None, 'tp')
- new_rope: bfloat16 [48, 480, 64], P('sp')
- attended: bfloat16 [48, 4096], P('sp', 'tp')
All inputs are finite; a program needn't handle non-finite values.
Results may differ from a plain program's by a relative error of at most 0.0085.
Values may be sent and summed in bfloat16 or wider, within the bound.
No kernel may reach another device: no remote copies, remote signals or barrier semaphores. Data moves between devices by JAX's collectives and lax.ppermute only.
A program may use at most 64 MiB of HBM per device.

v0:
```python
import jax
import jax.numpy as jnp
import numpy as np
from jax import lax
from jax.experimental import pallas as pl
from jax.experimental.pallas import tpu as pltpu
from jax.sharding import Mesh
from jax.sharding import PartitionSpec as P

PLAIN_KEY_WIDTH = 128
ROPE = 64
VALUE_WIDTH = 128
PAST_POSITIONS = 32768
TP = ("tp_0", "tp_1")
EXTRA = 16
TILE = 8
FACTOR = (PLAIN_KEY_WIDTH + ROPE) ** (-0.5)

epsilon = 1e-06
rope_theta = 10000.0

VMEM = pl.BlockSpec(memory_space=pltpu.VMEM)
HBM = pl.BlockSpec(memory_space=pltpu.HBM)
MIB = 1 << 20
f32, bf16 = jnp.float32, jnp.bfloat16
NT = (((1,), (1,)), ((), ()))


def mm(a, b):
    return jnp.dot(a, b, preferred_element_type=f32)


def mm_nt(a, b):
    return lax.dot_general(a, b, NT, preferred_element_type=f32)


def iota(shape, dim):
    return lax.broadcasted_iota(jnp.int32, shape, dim)


def by_head(row, width):
    shape = (TILE, row.shape[1])
    spread = jnp.broadcast_to(row.astype(f32), shape)
    return jnp.where(iota(shape, 1) // width == iota(shape, 0), spread, 0.0).astype(bf16)


def three(x):
    high = x.astype(bf16).astype(f32)
    rest = x - high
    middle = rest.astype(bf16).astype(f32)
    return high, middle, rest - middle


def pack_kernel(
    tokens_hbm,
    nope_hbm,
    turn_hbm,
    key_hbm,
    angle_ref,
    out_ref,
    angle_out_ref,
    nope_ref,
    turn_ref,
    key_ref,
    sem,
):
    needed = [
        pltpu.make_async_copy(source, target, sem.at[k])
        for k, (source, target) in enumerate(
            ((key_hbm, key_ref), (nope_hbm, nope_ref), (turn_hbm, turn_ref))
        )
    ]
    for copy in needed:
        copy.start()
    angle_out_ref[...] = angle_ref[...]
    rings, lines, half = out_ref.shape
    prompts = tokens_hbm.shape[1]
    copies = [pltpu.make_async_copy(tokens_hbm.at[:rings], out_ref.at[:, :prompts], sem.at[3])]
    last = prompts // EXTRA - 1
    for y in range(rings):
        third = jnp.minimum(lax.rem(y % (rings // 2) + lax.axis_index("sp"), rings // 2), last)
        part = pl.ds(pl.multiple_of(third * EXTRA, EXTRA), EXTRA)
        source = tokens_hbm.at[rings + y // (rings // 2), part]
        target = out_ref.at[y, prompts : prompts + EXTRA]
        copies.append(pltpu.make_async_copy(source, target, sem.at[4 + y]))
    for copy in copies:
        copy.start()
    for copy in needed:
        copy.wait()
    latent = mm_nt(by_head(nope_ref[...], PLAIN_KEY_WIDTH), key_ref[...])
    turn = turn_ref[...].astype(f32)
    blank = jnp.zeros((1, half - ROPE), f32)
    query = [latent[0:2, :half], latent[0:2, half:]]
    query += [jnp.concatenate([turn[:, h * ROPE : (h + 1) * ROPE], blank], axis=1) for h in (0, 1)]
    query.append(jnp.zeros((2, half), f32))
    query = jnp.concatenate(query, axis=0).astype(bf16)
    for y in range(rings):
        out_ref[y, lines - TILE :, :] = query
    for copy in copies:
        copy.wait()


def project_kernel(
    rows_ref,
    angle_ref,
    turn_down_hbm,
    gain_hbm,
    down_hbm,
    out_ref,
    line_ref,
    turn_down_ref,
    gain_ref,
    down_ref,
    sem,
):
    ranks, _, features = rows_ref.shape
    rings = ranks // 2
    prompts, tiles, lanes = out_ref.shape
    count = prompts + EXTRA
    width = down_ref.shape[1]
    copies = [
        pltpu.make_async_copy(turn_down_hbm, turn_down_ref, sem.at[0]),
        pltpu.make_async_copy(gain_hbm, gain_ref, sem.at[1]),
    ]
    for y in range(rings):
        part = pl.ds(2 * y * features, 2 * features)
        copies.append(pltpu.make_async_copy(down_hbm.at[part], down_ref.at[part], sem.at[2 + y]))
    for copy in copies:
        copy.start()
    line_ref[...] = jnp.zeros_like(line_ref)
    raw = jnp.zeros((count, width), f32)
    turned = jnp.zeros((count, ROPE), f32)
    copies[0].wait()
    copies[1].wait()
    for t in range(ranks):
        x = rows_ref[(t % 2) * rings + t // 2, :count, :]
        turned = turned + mm_nt(x, turn_down_ref[:, t * features : (t + 1) * features])
    for t in range(ranks):
        if t % 2 == 0:
            copies[2 + t // 2].wait()
        x = rows_ref[(t % 2) * rings + t // 2, :count, :]
        raw = raw + mm(x, down_ref[t * features : (t + 1) * features, :])
    scale = lax.rsqrt(jnp.mean(raw * raw, axis=-1, keepdims=True) + epsilon)
    latent = raw * scale * gain_ref[...]
    first, second = turned[:, : ROPE // 2], turned[:, ROPE // 2 :]
    full = iota((count, ROPE // 2), 0) < prompts
    cos = jnp.where(full, angle_ref[0, 0:1, :], angle_ref[0, 1:2, :])
    sin = jnp.where(full, angle_ref[1, 0:1, :], angle_ref[1, 1:2, :])
    turned = jnp.where(
        lax.axis_index("tp_1") == 0, first * cos - second * sin, first * sin + second * cos
    )
    half = width // 2
    own = jnp.where(lax.axis_index("tp_1") == 0, latent[:, :half], latent[:, half:])

    def repeated(x):
        return jnp.concatenate([x[prompts:]] * (prompts // EXTRA))

    parts = [own[:prompts, :lanes], own[:prompts, lanes:]]
    parts += [repeated(own[:, :lanes]), repeated(own[:, lanes:])]
    blank = jnp.zeros((prompts, lanes - ROPE), f32)
    parts.append(jnp.concatenate([turned[:prompts], repeated(turned), blank], axis=1))
    for k, part in enumerate(parts):
        line_ref[pl.ds(k, prompts, stride=tiles), :] = part
    out_ref[...] = line_ref[...].astype(bf16).reshape(out_ref.shape)


def past_kernel(rows_ref, cached_ref, past_ref, sums_ref, stats_ref):
    ranks, count, features = rows_ref.shape
    rings = ranks // 2
    width = cached_ref.shape[1]
    heads = 2 * ranks
    group = heads // rings
    lines = rows_ref[:, count - TILE :, :].reshape(ranks * TILE, features)
    shape = (heads, ranks * TILE)
    head, line = iota(shape, 0), iota(shape, 1)
    source = ((head // 2) % 2) * rings + head // 4

    def pick(first):
        wanted = source * TILE + first + head % 2
        return mm(jnp.where(line == wanted, 1.0, 0.0).astype(bf16), lines).astype(bf16)

    query = jnp.concatenate([pick(0), pick(2)], axis=1)
    turn = pick(4)[:, :ROPE]
    cached = cached_ref[...]
    score = (mm_nt(query, cached) + mm(turn, past_ref[...])) * FACTOR
    peak = jnp.max(score, axis=-1, keepdims=True)
    weight = jnp.exp(score - peak)
    total = jnp.sum(weight, axis=-1, keepdims=True)
    summed = mm(weight.astype(bf16), cached)
    high = summed.astype(bf16).astype(f32)
    low = summed - high

    shape = (heads, width // 2)
    column = iota(shape, 1) // 8 - 6 * (iota(shape, 0) % group)
    spread = jnp.zeros(shape, f32)
    for k, part in enumerate((*three(peak), *three(total))):
        spread = jnp.where(column == k, part, spread)
    shape = (rings, heads)
    wanted = jnp.where(iota(shape, 0) == iota(shape, 1) // group, 1.0, 0.0)
    numbers = mm(wanted.astype(bf16), spread.astype(bf16))
    for y in range(rings):
        at = slice(group * y, group * (y + 1))
        sums_ref[y] = jnp.concatenate([high[at], low[at]]).astype(bf16)
    stats_ref[...] = numbers


def chunk_kernel(lines_ref, sums_ref, stats_ref, out_ref, flat_ref):
    prompts, tiles, lanes = lines_ref.shape
    rings, lines, width = out_ref.shape
    turns = rings // 2
    flat_ref[...] = lines_ref[...].reshape(prompts * tiles, lanes).astype(f32)
    first = lax.rem(lax.axis_index("sp") // EXTRA + rings - lax.axis_index("tp_0"), turns)

    def some(k):
        return flat_ref[pl.ds(first * tiles + k, prompts // turns, stride=turns * tiles), :]

    full = [flat_ref[pl.ds(k, prompts, stride=tiles), :] for k in (0, 1, 4)]
    spare = EXTRA - prompts // turns
    stacked = jnp.concatenate(
        [
            jnp.concatenate(full[:2], axis=1),
            jnp.concatenate([some(2), some(3)], axis=1),
            jnp.zeros((spare, width // 2), f32),
        ]
    )
    count = stacked.shape[0] // 2
    latent = jnp.concatenate([stacked[:count], stacked[count:]], axis=1).astype(bf16)
    half = ROPE // 2
    turned = jnp.concatenate(
        [full[2][:, :half], some(4)[:, half:ROPE], jnp.zeros((spare, half), f32)]
    )
    turned = jnp.concatenate(
        [turned[TILE * k : TILE * (k + 1)] for k in range(2 * count // TILE)], axis=1
    )
    for y in range(rings):
        out_ref[y, :count, :] = latent
        out_ref[y, count : count + TILE, :] = sums_ref[y]
        numbers = jnp.concatenate(
            [stats_ref[y : y + 1, :], jnp.zeros((TILE - 1, width // 2), f32)]
        )
        out_ref[y, count + TILE :, :] = jnp.concatenate([turned, numbers], axis=1).astype(bf16)


def finish_kernel(
    both_ref,
    key_ref,
    value_hbm,
    nope_ref,
    turn_ref,
    place_ref,
    keys_ref,
    values_ref,
    rope_ref,
    out_ref,
    latent_ref,
    turned_ref,
    value_ref,
    sem,
):
    load = pltpu.make_async_copy(value_hbm, value_ref, sem)
    load.start()
    sources, lines, width = both_ref.shape
    rings = sources // 2
    count = lines - 2 * TILE
    rows = keys_ref.shape[0]
    group = 4
    half = ROPE // 2
    for y in range(rings):
        halves = []
        for c in range(2):
            source = c * rings + y
            columns = slice(c * width // 2, (c + 1) * width // 2)
            for upper in range(2):
                at = slice((2 * y + upper) * count, (2 * y + upper + 1) * count)
                latent_ref[at, columns] = both_ref[
                    source, :count, upper * width // 2 : (upper + 1) * width // 2
                ]
            packed = both_ref[source, count + TILE :, :].astype(f32)
            halves.append(
                jnp.concatenate(
                    [packed[:, half * k : half * (k + 1)] for k in range(2 * count // TILE)]
                )
            )
        at = slice(2 * y * count, 2 * (y + 1) * count)
        turned_ref[at, :] = jnp.concatenate(halves, axis=1).astype(bf16)

    third = lax.axis_index("sp") // EXTRA
    place = place_ref[0:1, :]
    for k in range(1, place_ref.shape[0]):
        place = jnp.where(third == k, place_ref[k : k + 1, :], place)
    held = latent_ref.shape[0]
    move = jnp.where(iota((rows, held), 0) == place, 1.0, 0.0).astype(bf16)
    latent = mm(move, latent_ref[...]).astype(bf16)
    turned = mm(move, turned_ref[...]).astype(bf16)
    keys = mm(latent, key_ref[...]).astype(bf16)
    keys_ref[...] = keys
    load.wait()
    values = mm(latent, value_ref[...]).astype(bf16)
    values_ref[...] = values
    same = jnp.where(iota((ROPE, ROPE), 0) == iota((ROPE, ROPE), 1), 1.0, 0.0).astype(bf16)
    rope = mm_nt(same, turned).astype(bf16)
    rope_ref[...] = rope

    nope = by_head(nope_ref[...], PLAIN_KEY_WIDTH)
    turn = by_head(turn_ref[...], ROPE)
    score = (mm_nt(nope, keys) + mm(turn, jnp.concatenate([rope, rope], axis=0))) * FACTOR

    shape = (group, width // 2)
    place = iota(shape, 1) // 8 - 6 * iota(shape, 0)
    mine = [(iota(shape, 1) % 8 == 0) & (place >= k) & (place < k + 3) for k in (0, 3)]
    peaks, totals = [], []
    for source in range(sources):
        numbers = both_ref[source, count + TILE :, width // 2 :].astype(f32)[:1]
        for found, where in zip((peaks, totals), mine):
            found.append(jnp.sum(jnp.where(where, numbers, 0.0), axis=-1, keepdims=True))
    past_peak = peaks[0]
    for x in peaks[1:]:
        past_peak = jnp.maximum(past_peak, x)
    past_total = jnp.zeros((group, 1), f32)
    past_sum = jnp.zeros((TILE, width), f32)
    for k in range(sources):
        share = jnp.exp(peaks[k] - past_peak)
        past_total = past_total + totals[k] * share
        sums = both_ref[k, count : count + TILE, :].astype(f32)
        past_sum = past_sum + sums * jnp.concatenate([share, share])
    past_sum = past_sum[:group] + past_sum[group:]

    def own(x):
        half = group // 2
        mine = jnp.where(lax.axis_index("tp_1") == 0, x[:half], x[half:])
        return jnp.concatenate([mine, jnp.zeros((TILE - half, x.shape[1]), f32)])

    past_peak, past_total, past_sum = own(past_peak), own(past_total), own(past_sum)
    peak = jnp.maximum(past_peak, jnp.max(score, axis=-1, keepdims=True))
    share = jnp.exp(past_peak - peak)
    weight = jnp.exp(score - peak)
    denominator = past_total * share + jnp.sum(weight, axis=-1, keepdims=True)
    result = mm((past_sum * share).astype(bf16), value_ref[...]) + mm(weight.astype(bf16), values)
    result = result / denominator
    shape = result.shape
    result = jnp.where(iota(shape, 1) // VALUE_WIDTH == iota(shape, 0), result, 0.0)
    out_ref[...] = jnp.sum(result, axis=0, keepdims=True).astype(bf16)


def shaped(shape, dtype=bf16):
    return jax.ShapeDtypeStruct(shape, dtype)


def limit(mib):
    return pltpu.CompilerParams(vmem_limit_bytes=mib * MIB)


def pinned(x):
    return pltpu.with_memory_space_constraint(x, pltpu.HBM)


def on_device(
    tokens,
    latent_down_weight,
    w_rope_key,
    latent_norm_gain,
    key_up_weight,
    value_up_weight,
    cached_latent_rows,
    past_rope,
    query_nope,
    query_rope,
):
    prompts, per_device, features = tokens.shape
    width = latent_down_weight.shape[1]
    row_count = prompts * per_device
    rings = lax.axis_size("tp_0")
    ring = lax.axis_index("tp_0")
    device = lax.axis_index("sp")

    places = jnp.stack([ring, rings + ring // (rings // 2)])
    positions = (PAST_POSITIONS + device * per_device + places).astype(f32)
    halfway = ROPE // 2
    frequency = rope_theta ** (-jnp.arange(halfway, dtype=f32) / halfway)
    angles = positions[:, None] * frequency

    turns = jnp.stack([jnp.cos(angles), jnp.sin(angles)])
    sources = (query_nope, query_rope, key_up_weight)
    outgoing, turns = pl.pallas_call(
        pack_kernel,
        out_shape=(shaped((rings, prompts + EXTRA + TILE, features)), shaped(turns.shape, f32)),
        in_specs=[HBM] * 4 + [VMEM],
        out_specs=(VMEM, VMEM),
        scratch_shapes=[pltpu.VMEM(x.shape, bf16) for x in sources]
        + [pltpu.SemaphoreType.DMA((4 + rings,))],
        name="pack",
        compiler_params=limit(4),
    )(pinned(tokens.transpose(1, 0, 2)), *(pinned(x) for x in sources), turns)
    rows = lax.all_to_all(outgoing, "tp_0", split_axis=0, concat_axis=0, tiled=True)
    rows = lax.all_gather(rows, "tp_1", axis=0, tiled=True)

    lanes = 128
    sources = (w_rope_key.T, latent_norm_gain[None], latent_down_weight)
    lines = pl.pallas_call(
        project_kernel,
        out_shape=shaped((prompts, TILE, lanes)),
        in_specs=[VMEM] * 2 + [HBM] * 3,
        out_specs=VMEM,
        scratch_shapes=[pltpu.VMEM((prompts * TILE, lanes), f32)]
        + [pltpu.VMEM(x.shape, x.dtype) for x in sources]
        + [pltpu.SemaphoreType.DMA((rings + 2,))],
        name="project",
        compiler_params=limit(12),
    )(rows, turns, *(pinned(x) for x in sources))
    arrived = lax.all_to_all(lines, "sp", split_axis=0, concat_axis=0, tiled=True)

    sums, stats = pl.pallas_call(
        past_kernel,
        out_shape=(shaped((rings, TILE, width)), shaped((rings, width // 2), f32)),
        in_specs=[VMEM] * 3,
        out_specs=(VMEM, VMEM),
        name="past",
        compiler_params=limit(4),
        cost_estimate=pl.CostEstimate(
            flops=300_000_000, bytes_accessed=4 * MIB, transcendentals=65536
        ),
    )(rows, cached_latent_rows[0], past_rope[0].T)

    count = prompts + EXTRA
    chunk = pl.pallas_call(
        chunk_kernel,
        out_shape=shaped((rings, count // 2 + 2 * TILE, width)),
        in_specs=[VMEM] * 3,
        out_specs=VMEM,
        scratch_shapes=[pltpu.VMEM((prompts * TILE, lanes), f32)],
        name="chunk",
        compiler_params=limit(4),
    )(arrived, sums, stats)
    got = lax.all_to_all(chunk, "tp_0", split_axis=0, concat_axis=0, tiled=True)
    both = lax.all_gather(got, "tp_1", axis=0, tiled=True)

    turns_of = rings // 2
    y, k = np.divmod(np.arange(rings * count), count)
    tables = []
    for third in range(prompts // EXTRA):
        source = turns_of * (k - prompts) + (third - y) % turns_of
        extra = np.where(source < prompts, per_device * source + rings + y // turns_of, -1)
        tables.append(np.where(k < prompts, per_device * k + y, extra))
    keys, values, rope, attended = pl.pallas_call(
        finish_kernel,
        out_shape=(
            shaped((row_count, key_up_weight.shape[1])),
            shaped((row_count, value_up_weight.shape[1])),
            shaped((ROPE, row_count)),
            shaped((1, value_up_weight.shape[1])),
        ),
        in_specs=[VMEM, VMEM, HBM, VMEM, VMEM, VMEM],
        out_specs=(VMEM,) * 4,
        scratch_shapes=[
            pltpu.VMEM((rings * count, width), bf16),
            pltpu.VMEM((rings * count, ROPE), bf16),
            pltpu.VMEM(value_up_weight.shape, bf16),
            pltpu.SemaphoreType.DMA(()),
        ],
        name="finish",
        compiler_params=limit(8),
    )(
        both,
        key_up_weight,
        pinned(value_up_weight),
        query_nope,
        query_rope,
        jnp.asarray(np.stack(tables), jnp.int32),
    )
    return (keys[None], values[None], rope.T[None], attended)


def solution(mesh):
    split = Mesh(mesh.devices.reshape(mesh.shape["sp"], 8, 2), ("sp", "tp_0", "tp_1"))
    return jax.shard_map(
        on_device,
        mesh=split,
        in_specs=(
            P(None, "sp", TP),
            P(),
            P(),
            P(),
            P(None, TP),
            P(None, TP),
            P("sp", TP, None),
            P("sp", TP, None),
            P("sp", TP),
            P("sp", TP),
        ),
        out_specs=(P("sp", None, TP), P("sp", None, TP), P("sp", None, None), P("sp", TP)),
        check_vma=False,
    )
```

profile of v0, /device:TPU:1, one launch (start us, length us, event | category | flops | bytes accessed | tf_op | source)
XLA Modules:
  0.0 81.7 jit_solution(14028461959895123289)
XLA Ops:
  0.6 0.0 copy-start.2
  0.6 0.0 copy-start
  0.7 0.1 fusion
  0.8 0.1 multiply_cosine_fusion
  0.9 1.4 %pack.1 = (bf16[8,72,256]{2,1,0:T(8,128)(2,1)S(1)}, f32[2,2,32]{2,1,0:T(2,128)S(1)}) custom-call(bf16[10,48,256]{2,1,0:T(8,128)(2,1)} %bitcast.17, bf16[1,256]{1,0:T(2,128)(2,1)} %nope_ref.1, bf16[1,128]{1,0:T(2,128)(2,1)} %turn_ref.1, bf16[512,256]{1,0:T(8,128)(2,1)} %key_ref.1, f32[2,2,32]{2,1,0:T(2,128)S(1)} %pad_maximum_fusion.angle_ref), custom_call_target="tpu_custom_call" | custom-call | tf_op jit(solution)/shard_map/pack/pallas_call | solution.py:384
  2.3 17.1 %all_to_all.15 = bf16[8,72,256]{2,1,0:T(8,128)(2,1)S(1)} all-to-all(bf16[8,72,256]{2,1,0:T(8,128)(2,1)S(1)} %get-tuple-element.12), channel_id=1, replica_groups=mesh['sp'=48,'tp_0'=8,'tp_1'=2] {'tp_0'}, dimensions={0} | all-to-all | bytes 589824 | tf_op jit(solution)/shard_map/all_to_all | solution.py:394
  19.4 8.4 %all_gather.6.rows_ref = bf16[16,72,256]{2,1,0:T(8,128)(2,1)S(1)} all-gather(bf16[8,72,256]{2,1,0:T(8,128)(2,1)S(1)} %all_to_all.15), channel_id=1, replica_groups=mesh['sp'=48,'tp_0'=8,'tp_1'=2] {'tp_1'}, dimensions={0}, use_global_device_ids=true | all-gather | bytes 884736 | tf_op jit(solution)/shard_map/all_gather | solution.py:395
  27.8 3.8 %project.1 = bf16[48,8,128]{2,1,0:T(8,128)(2,1)} custom-call(bf16[16,72,256]{2,1,0:T(8,128)(2,1)S(1)} %all_gather.6.rows_ref, f32[2,2,32]{2,1,0:T(2,128)S(1)} %get-tuple-element.13.angle_ref, bf16[64,4096]{1,0:T(8,128)(2,1)} %bitcast.16, f32[1,512]{1,0:T(1,128)} %bitcast.18, bf16[4096,512]{1,0:T(8,128)(2,1)} %down_hbm.1), custom_call_target="tpu_custom_call" | custom-call | tf_op jit(solution)/shard_map/project/pallas_call | solution.py:399
  31.6 0.0 copy-start.1
  31.7 0.0 copy-start.3
  31.7 0.0 copy-start.4
  31.7 0.0 copy-start.5
  31.7 15.4 %all-to-all-start.1 = ((bf16[48,8,128]{2,1,0:T(8,128)(2,1)}), bf16[48,8,128]{2,1,0:T(8,128)(2,1)S(1)}, u32[]{:S(2)}, u32[]{:S(2)}) async-start(bf16[48,8,128]{2,1,0:T(8,128)(2,1)} %project.1), calls=%async_computation.1 | async-start | bytes 196608 | tf_op jit(solution)/shard_map/all_to_all | solution.py:410
  47.1 0.0 copy-done.2
  47.2 0.0 copy-done
  47.2 1.9 %past.1 = (bf16[8,8,512]{2,1,0:T(8,128)(2,1)S(1)}, f32[8,256]{1,0:T(8,128)S(1)}) custom-call(bf16[16,72,256]{2,1,0:T(8,128)(2,1)S(1)} %all_gather.6.rows_ref, bf16[2048,512]{1,0:T(8,128)(2,1)S(1)} %bitcast.14, bf16[64,2048]{1,0:T(8,128)(2,1)S(1)} %bitcast.15), custom_call_target="tpu_custom_call" | custom-call | flops 300000000 | bytes 4194304 | tf_op jit(solution)/shard_map/past/pallas_call | solution.py:412
  49.0 9.5 %all-to-all-done.1.lines_ref = bf16[48,8,128]{2,1,0:T(8,128)(2,1)S(1)} async-done(((bf16[48,8,128]{2,1,0:T(8,128)(2,1)}), bf16[48,8,128]{2,1,0:T(8,128)(2,1)S(1)}, u32[]{:S(2)}, u32[]{:S(2)}) %all-to-all-start.1) | async-done | bytes 98336 | tf_op jit(solution)/shard_map/all_to_all | solution.py:410
  58.5 0.2 chunk.1
  58.7 14.1 %all_to_all.16 = bf16[8,48,512]{2,1,0:T(8,128)(2,1)S(1)} all-to-all(bf16[8,48,512]{2,1,0:T(8,128)(2,1)S(1)} %chunk.1), channel_id=1, replica_groups=mesh['sp'=48,'tp_0'=8,'tp_1'=2] {'tp_0'}, dimensions={0} | all-to-all | bytes 786432 | tf_op jit(solution)/shard_map/all_to_all | solution.py:434
  72.8 5.9 %all_gather.7.both_ref = bf16[16,48,512]{2,1,0:T(8,128)(2,1)S(1)} all-gather(bf16[8,48,512]{2,1,0:T(8,128)(2,1)S(1)} %all_to_all.16), channel_id=1, replica_groups=mesh['sp'=48,'tp_0'=8,'tp_1'=2] {'tp_1'}, dimensions={0}, use_global_device_ids=true | all-gather | bytes 1179648 | tf_op jit(solution)/shard_map/all_gather | solution.py:435
  78.7 0.0 copy-done.1
  78.7 0.0 copy-done.3
  78.7 0.0 copy-done.4
  78.7 0.0 copy-done.5
  78.7 2.9 %finish.1 = (bf16[480,256]{1,0:T(8,128)(2,1)}, bf16[480,256]{1,0:T(8,128)(2,1)}, bf16[64,480]{1,0:T(8,128)(2,1)}, bf16[1,256]{1,0:T(2,128)(2,1)}) custom-call(bf16[16,48,512]{2,1,0:T(8,128)(2,1)S(1)} %all_gather.7.both_ref, bf16[512,256]{1,0:T(8,128)(2,1)S(1)} %copy-done.1, bf16[512,256]{1,0:T(8,128)(2,1)} %value_hbm.1, bf16[1,256]{1,0:T(2,128)(2,1)S(1)} %copy-done.4, ...), custom_call_target="tpu_custom_call" | custom-call | tf_op jit(solution)/shard_map/finish/pallas_call | solution.py:444
  (2 shorter events, 0.0 us)
Async XLA Ops:
  0.6 46.5 %copy-start.2 = (bf16[1,2048,64]{1,2,0:T(8,128)(2,1)S(1)}, bf16[1,2048,64]{1,2,0:T(8,128)(2,1)}, u32[]{:S(2)}) copy-start(bf16[1,2048,64]{1,2,0:T(8,128)(2,1)} %param.18) | copy-start | bytes 786436
  0.6 46.5 %copy-start = (bf16[1,2048,512]{2,1,0:T(8,128)(2,1)S(1)}, bf16[1,2048,512]{2,1,0:T(8,128)(2,1)}, u32[]{:S(2)}) copy-start(bf16[1,2048,512]{2,1,0:T(8,128)(2,1)} %param.17) | copy-start | bytes 6291460
  31.6 47.1 %copy-start.1 = (bf16[512,256]{1,0:T(8,128)(2,1)S(1)}, bf16[512,256]{1,0:T(8,128)(2,1)}, u32[]{:S(2)}) copy-start(bf16[512,256]{1,0:T(8,128)(2,1)} %key_ref.1) | copy-start | bytes 786436
  31.7 47.1 %copy-start.3 = (s32[3,512]{1,0:T(4,128)S(1)}, s32[3,512]{1,0:T(4,128)}, u32[]{:S(2)}) copy-start(s32[3,512]{1,0:T(4,128)} %constant.40.clone.place_ref) | copy-start | bytes 18436
  31.7 47.1 %copy-start.4 = (bf16[1,256]{1,0:T(2,128)(2,1)S(1)}, bf16[1,256]{1,0:T(2,128)(2,1)}, u32[]{:S(2)}) copy-start(bf16[1,256]{1,0:T(2,128)(2,1)} %nope_ref.1) | copy-start | bytes 1540
  31.7 47.1 %copy-start.5 = (bf16[1,128]{1,0:T(2,128)(2,1)S(1)}, bf16[1,128]{1,0:T(2,128)(2,1)}, u32[]{:S(2)}) copy-start(bf16[1,128]{1,0:T(2,128)(2,1)} %turn_ref.1) | copy-start | bytes 772
  31.7 26.8 %all-to-all-start.1 = ((bf16[48,8,128]{2,1,0:T(8,128)(2,1)}), bf16[48,8,128]{2,1,0:T(8,128)(2,1)S(1)}, u32[]{:S(2)}, u32[]{:S(2)}) async-start(bf16[48,8,128]{2,1,0:T(8,128)(2,1)} %project.1), calls=%async_computation.1 | async-start | bytes 196608 | tf_op jit(solution)/shard_map/all_to_all | solution.py:410
where the time goes:
time: 82 us; the launch traced here: 81.7 us
  blocking collectives  45.5 us (55%)
  starting transfers between devices  15.4 us (19%)
  Pallas kernels  10.2 us (12%)
  waiting for transfers between devices  9.5 us (12%)
    all_to_all x1, blocking collectives, on_device(): lax.all_to_all(outgoing, 'tp_0', split_axis=0, concat_axis=0, tiled=True)  17.1 us
    all_to_all x1, starting transfers between devices, on_device(): lax.all_to_all(lines, 'sp', split_axis=0, concat_axis=0, tiled=True)  15.4 us
    all_to_all x1, blocking collectives, on_device(): got = lax.all_to_all(chunk, 'tp_0', split_axis=0, concat_axis=0, tiled=True)  14.1 us
    all_to_all x1, waiting for transfers between devices, on_device(): lax.all_to_all(lines, 'sp', split_axis=0, concat_axis=0, tiled=True)  9.5 us
    all_gather x1, blocking collectives, on_device(): rows = lax.all_gather(rows, 'tp_1', axis=0, tiled=True)  8.4 us
    all_gather x1, blocking collectives, on_device(): both = lax.all_gather(got, 'tp_1', axis=0, tiled=True)  5.94 us
    pallas_call x1, Pallas kernels, on_device(): pl.pallas_call(project_kernel, out_shape=shaped((prompts, TILE, lanes)),...  3.81 us
    pallas_call x1, Pallas kernels, on_device(): pl.pallas_call(finish_kernel, out_shape=(shaped((row_count, key_up_weight...  2.93 us
  transfers between devices with their start and end apart: 1, of which 1 were waited for; matrix products, arithmetic and copies ran while one was open for 0% of the time, Pallas kernels for 2%

commit v1 on v0

--- a/solution.py
+++ b/solution.py
@@ -103,10 +103,14 @@
 def project_kernel(
     rows_ref,
     angle_ref,
+    cached_ref,
+    past_ref,
     turn_down_hbm,
     gain_hbm,
     down_hbm,
     out_ref,
+    sums_ref,
+    stats_ref,
     line_ref,
     turn_down_ref,
     gain_ref,
@@ -128,6 +132,7 @@
     for copy in copies:
         copy.start()
     line_ref[...] = jnp.zeros_like(line_ref)
+    read_cached(rows_ref, cached_ref, past_ref, sums_ref, stats_ref)
     raw = jnp.zeros((count, width), f32)
     turned = jnp.zeros((count, ROPE), f32)
     copies[0].wait()
@@ -164,7 +169,7 @@
     out_ref[...] = line_ref[...].astype(bf16).reshape(out_ref.shape)
 
 
-def past_kernel(rows_ref, cached_ref, past_ref, sums_ref, stats_ref):
+def read_cached(rows_ref, cached_ref, past_ref, sums_ref, stats_ref):
     ranks, count, features = rows_ref.shape
     rings = ranks // 2
     width = cached_ref.shape[1]
@@ -396,30 +401,22 @@
 
     lanes = 128
     sources = (w_rope_key.T, latent_norm_gain[None], latent_down_weight)
-    lines = pl.pallas_call(
+    lines, sums, stats = pl.pallas_call(
         project_kernel,
-        out_shape=shaped((prompts, TILE, lanes)),
-        in_specs=[VMEM] * 2 + [HBM] * 3,
-        out_specs=VMEM,
+        out_shape=(
+            shaped((prompts, TILE, lanes)),
+            shaped((rings, TILE, width)),
+            shaped((rings, width // 2), f32),
+        ),
+        in_specs=[VMEM] * 4 + [HBM] * 3,
+        out_specs=(VMEM,) * 3,
         scratch_shapes=[pltpu.VMEM((prompts * TILE, lanes), f32)]
         + [pltpu.VMEM(x.shape, x.dtype) for x in sources]
         + [pltpu.SemaphoreType.DMA((rings + 2,))],
         name="project",
         compiler_params=limit(12),
-    )(rows, turns, *(pinned(x) for x in sources))
+    )(rows, turns, cached_latent_rows[0], past_rope[0].T, *(pinned(x) for x in sources))
     arrived = lax.all_to_all(lines, "sp", split_axis=0, concat_axis=0, tiled=True)
-
-    sums, stats = pl.pallas_call(
-        past_kernel,
-        out_shape=(shaped((rings, TILE, width)), shaped((rings, width // 2), f32)),
-        in_specs=[VMEM] * 3,
-        out_specs=(VMEM, VMEM),
-        name="past",
-        compiler_params=limit(4),
-        cost_estimate=pl.CostEstimate(
-            flops=300_000_000, bytes_accessed=4 * MIB, transcendentals=65536
-        ),
-    )(rows, cached_latent_rows[0], past_rope[0].T)
 
     count = prompts + EXTRA
     chunk = pl.pallas_call(

time: 82 us -> 83.5 us (1.018)
  blocking collectives: 45.5 us -> 72 us
  starting transfers between devices: 15.4 us -> 0 us
  waiting for transfers between devices: 9.5 us -> 0 us
  Pallas kernels: 10.2 us -> 7.67 us
  local copies, waits for them, and re-layouts: 0.03 us -> 2.55 us
    all_to_all x0 -> x1, blocking collectives: none -> 26.5 us  [on_device(): lax.all_to_all(lines, 'sp', split_axis=0, concat_axis=0, tiled=True)]
    all_to_all x1 -> x0, starting transfers between devices: 15.4 us -> none  [on_device(): lax.all_to_all(lines, 'sp', split_axis=0, concat_axis=0, tiled=True)]
    all_to_all x1 -> x0, waiting for transfers between devices: 9.5 us -> none  [on_device(): lax.all_to_all(lines, 'sp', split_axis=0, concat_axis=0, tiled=True)]
    unnamed x12, local copies, waits for them, and re-layouts: 0.03 us -> 2.55 us
    pallas_call x2 -> x1, Pallas kernels: 5.67 us -> 3.28 us  [on_device(): pl.pallas_call(project_kernel, out_shape=(shaped((prompts, TILE, lanes)),...]
  transfers between devices with their start and end apart: 1 -> 0, of which waited for: 1 -> 0; matrix products, arithmetic and copies ran while one was open for 0% -> 0% of each run, Pallas kernels for 2% -> 0%
where the time goes in v1:
time: 83.5 us; the launch traced here: 83.2 us
  blocking collectives  72 us (86%)
  Pallas kernels  7.67 us (9%)
  local copies, waits for them, and re-layouts  2.55 us (3%)
    all_to_all x1, blocking collectives, on_device(): lax.all_to_all(lines, 'sp', split_axis=0, concat_axis=0, tiled=True)  26.5 us
    all_to_all x1, blocking collectives, on_device(): lax.all_to_all(outgoing, 'tp_0', split_axis=0, concat_axis=0, tiled=True)  17.1 us
    all_to_all x1, blocking collectives, on_device(): got = lax.all_to_all(chunk, 'tp_0', split_axis=0, concat_axis=0, tiled=True)  14.1 us
    all_gather x1, blocking collectives, on_device(): rows = lax.all_gather(rows, 'tp_1', axis=0, tiled=True)  8.4 us
    all_gather x1, blocking collectives, on_device(): both = lax.all_gather(got, 'tp_1', axis=0, tiled=True)  5.94 us
    pallas_call x1, Pallas kernels, on_device(): pl.pallas_call(project_kernel, out_shape=(shaped((prompts, TILE, lanes)),...  3.28 us
    pallas_call x1, Pallas kernels, on_device(): pl.pallas_call(finish_kernel, out_shape=(shaped((row_count, key_up_weight...  2.94 us
    unnamed x12, local copies, waits for them, and re-layouts  2.55 us

profile of v1, /device:TPU:1, one launch (start us, length us, event | category | flops | bytes accessed | tf_op | source)
XLA Modules:
  0.0 83.2 jit_solution(10871443659530153965)
XLA Ops:
  0.7 0.1 fusion
  0.8 0.1 multiply_cosine_fusion
  0.9 1.3 %pack.1 = (bf16[8,72,256]{2,1,0:T(8,128)(2,1)S(1)}, f32[2,2,32]{2,1,0:T(2,128)S(1)}) custom-call(bf16[10,48,256]{2,1,0:T(8,128)(2,1)} %bitcast.17, bf16[1,256]{1,0:T(2,128)(2,1)} %nope_ref.1, bf16[1,128]{1,0:T(2,128)(2,1)} %turn_ref.1, bf16[512,256]{1,0:T(8,128)(2,1)} %key_ref.1, f32[2,2,32]{2,1,0:T(2,128)S(1)} %pad_maximum_fusion.angle_ref), custom_call_target="tpu_custom_call" | custom-call | tf_op jit(solution)/shard_map/pack/pallas_call | solution.py:389
  2.2 17.1 %all_to_all.15 = bf16[8,72,256]{2,1,0:T(8,128)(2,1)S(1)} all-to-all(bf16[8,72,256]{2,1,0:T(8,128)(2,1)S(1)} %get-tuple-element.13), channel_id=1, replica_groups=mesh['sp'=48,'tp_0'=8,'tp_1'=2] {'tp_0'}, dimensions={0} | all-to-all | bytes 589824 | tf_op jit(solution)/shard_map/all_to_all | solution.py:399
  19.3 8.4 %all_gather.6.rows_ref = bf16[16,72,256]{2,1,0:T(8,128)(2,1)S(1)} all-gather(bf16[8,72,256]{2,1,0:T(8,128)(2,1)S(1)} %all_to_all.15), channel_id=1, replica_groups=mesh['sp'=48,'tp_0'=8,'tp_1'=2] {'tp_1'}, dimensions={0}, use_global_device_ids=true | all-gather | bytes 884736 | tf_op jit(solution)/shard_map/all_gather | solution.py:400
  27.7 0.0 copy-start
  27.7 1.6 %copy-done = bf16[1,2048,512]{2,1,0:T(8,128)(2,1)S(1)} copy-done((bf16[1,2048,512]{2,1,0:T(8,128)(2,1)S(1)}, bf16[1,2048,512]{2,1,0:T(8,128)(2,1)}, u32[]{:S(2)}) %copy-start) | copy-done | bytes 2097176
  29.3 0.0 copy-start.2
  29.3 0.9 %copy-done.2 = bf16[1,2048,64]{1,2,0:T(8,128)(2,1)S(1)} copy-done((bf16[1,2048,64]{1,2,0:T(8,128)(2,1)S(1)}, bf16[1,2048,64]{1,2,0:T(8,128)(2,1)}, u32[]{:S(2)}) %copy-start.2) | copy-done | bytes 262168
  30.2 0.0 copy-start.1
  30.2 0.0 copy-start.3
  30.2 0.0 copy-start.4
  30.2 0.0 copy-start.5
  30.2 3.3 %project.1 = (bf16[48,8,128]{2,1,0:T(8,128)(2,1)S(1)}, bf16[8,8,512]{2,1,0:T(8,128)(2,1)S(1)}, f32[8,256]{1,0:T(8,128)S(1)}) custom-call(bf16[16,72,256]{2,1,0:T(8,128)(2,1)S(1)} %all_gather.6.rows_ref, f32[2,2,32]{2,1,0:T(2,128)S(1)} %get-tuple-element.14.angle_ref, bf16[2048,512]{1,0:T(8,128)(2,1)S(1)} %bitcast.14, bf16[64,2048]{1,0:T(8,128)(2,1)S(1)} %bitcast.15, ...), custom_call_target="tpu_custom_call" | custom-call | tf_op jit(solution)/shard_map/project/pallas_call | solution.py:404
  33.5 26.5 %all_to_all.16.lines_ref = bf16[48,8,128]{2,1,0:T(8,128)(2,1)S(1)} all-to-all(bf16[48,8,128]{2,1,0:T(8,128)(2,1)S(1)} %get-tuple-element.15), channel_id=1, replica_groups=mesh['sp'=48,'tp_0'=8,'tp_1'=2] {'sp'}, dimensions={0} | all-to-all | bytes 196608 | tf_op jit(solution)/shard_map/all_to_all | solution.py:419
  60.0 0.2 chunk.1
  60.2 14.1 %all_to_all.17 = bf16[8,48,512]{2,1,0:T(8,128)(2,1)S(1)} all-to-all(bf16[8,48,512]{2,1,0:T(8,128)(2,1)S(1)} %chunk.1), channel_id=1, replica_groups=mesh['sp'=48,'tp_0'=8,'tp_1'=2] {'tp_0'}, dimensions={0} | all-to-all | bytes 786432 | tf_op jit(solution)/shard_map/all_to_all | solution.py:431
  74.3 5.9 %all_gather.7.both_ref = bf16[16,48,512]{2,1,0:T(8,128)(2,1)S(1)} all-gather(bf16[8,48,512]{2,1,0:T(8,128)(2,1)S(1)} %all_to_all.17), channel_id=1, replica_groups=mesh['sp'=48,'tp_0'=8,'tp_1'=2] {'tp_1'}, dimensions={0}, use_global_device_ids=true | all-gather | bytes 1179648 | tf_op jit(solution)/shard_map/all_gather | solution.py:432
  80.2 0.0 copy-done.1
  80.2 0.0 copy-done.3
  80.2 0.0 copy-done.4
  80.2 0.0 copy-done.5
  80.2 2.9 %finish.1 = (bf16[480,256]{1,0:T(8,128)(2,1)}, bf16[480,256]{1,0:T(8,128)(2,1)}, bf16[64,480]{1,0:T(8,128)(2,1)}, bf16[1,256]{1,0:T(2,128)(2,1)}) custom-call(bf16[16,48,512]{2,1,0:T(8,128)(2,1)S(1)} %all_gather.7.both_ref, bf16[512,256]{1,0:T(8,128)(2,1)S(1)} %copy-done.1, bf16[512,256]{1,0:T(8,128)(2,1)} %value_hbm.1, bf16[1,256]{1,0:T(2,128)(2,1)S(1)} %copy-done.4, ...), custom_call_target="tpu_custom_call" | custom-call | tf_op jit(solution)/shard_map/finish/pallas_call | solution.py:441
  (2 shorter events, 0.0 us)
Async XLA Ops:
  27.7 1.6 %copy-start = (bf16[1,2048,512]{2,1,0:T(8,128)(2,1)S(1)}, bf16[1,2048,512]{2,1,0:T(8,128)(2,1)}, u32[]{:S(2)}) copy-start(bf16[1,2048,512]{2,1,0:T(8,128)(2,1)} %param.17) | copy-start | bytes 6291460
  29.3 0.9 %copy-start.2 = (bf16[1,2048,64]{1,2,0:T(8,128)(2,1)S(1)}, bf16[1,2048,64]{1,2,0:T(8,128)(2,1)}, u32[]{:S(2)}) copy-start(bf16[1,2048,64]{1,2,0:T(8,128)(2,1)} %param.18) | copy-start | bytes 786436
  30.2 50.0 %copy-start.1 = (bf16[512,256]{1,0:T(8,128)(2,1)S(1)}, bf16[512,256]{1,0:T(8,128)(2,1)}, u32[]{:S(2)}) copy-start(bf16[512,256]{1,0:T(8,128)(2,1)} %key_ref.1) | copy-start | bytes 786436
  30.2 50.0 %copy-start.3 = (s32[3,512]{1,0:T(4,128)S(1)}, s32[3,512]{1,0:T(4,128)}, u32[]{:S(2)}) copy-start(s32[3,512]{1,0:T(4,128)} %constant.40.clone.place_ref) | copy-start | bytes 18436
  30.2 50.0 %copy-start.4 = (bf16[1,256]{1,0:T(2,128)(2,1)S(1)}, bf16[1,256]{1,0:T(2,128)(2,1)}, u32[]{:S(2)}) copy-start(bf16[1,256]{1,0:T(2,128)(2,1)} %nope_ref.1) | copy-start | bytes 1540
  30.2 50.0 %copy-start.5 = (bf16[1,128]{1,0:T(2,128)(2,1)S(1)}, bf16[1,128]{1,0:T(2,128)(2,1)}, u32[]{:S(2)}) copy-start(bf16[1,128]{1,0:T(2,128)(2,1)} %turn_ref.1) | copy-start | bytes 772

commit v2 on v1

--- a/solution.py
+++ b/solution.py
@@ -21,6 +21,7 @@
 
 VMEM = pl.BlockSpec(memory_space=pltpu.VMEM)
 HBM = pl.BlockSpec(memory_space=pltpu.HBM)
+ANY = pl.BlockSpec(memory_space=pl.ANY)
 MIB = 1 << 20
 f32, bf16 = jnp.float32, jnp.bfloat16
 NT = (((1,), (1,)), ((), ()))
@@ -56,9 +57,13 @@
     nope_hbm,
     turn_hbm,
     key_hbm,
+    cached_hbm,
+    past_hbm,
     angle_ref,
     out_ref,
     angle_out_ref,
+    cached_ref,
+    past_ref,
     nope_ref,
     turn_ref,
     key_ref,
@@ -83,6 +88,8 @@
         source = tokens_hbm.at[rings + y // (rings // 2), part]
         target = out_ref.at[y, prompts : prompts + EXTRA]
         copies.append(pltpu.make_async_copy(source, target, sem.at[4 + y]))
+    copies.append(pltpu.make_async_copy(past_hbm, past_ref, sem.at[4 + rings]))
+    copies.append(pltpu.make_async_copy(cached_hbm, cached_ref, sem.at[5 + rings]))
     for copy in copies:
         copy.start()
     for copy in needed:
@@ -386,16 +393,21 @@
 
     turns = jnp.stack([jnp.cos(angles), jnp.sin(angles)])
     sources = (query_nope, query_rope, key_up_weight)
-    outgoing, turns = pl.pallas_call(
+    past = (cached_latent_rows[0], past_rope[0].T)
+    outgoing, turns, *past = pl.pallas_call(
         pack_kernel,
-        out_shape=(shaped((rings, prompts + EXTRA + TILE, features)), shaped(turns.shape, f32)),
-        in_specs=[HBM] * 4 + [VMEM],
-        out_specs=(VMEM, VMEM),
+        out_shape=(
+            shaped((rings, prompts + EXTRA + TILE, features)),
+            shaped(turns.shape, f32),
+            *(shaped(x.shape) for x in past),
+        ),
+        in_specs=[HBM] * 6 + [VMEM],
+        out_specs=(VMEM, VMEM, ANY, ANY),
         scratch_shapes=[pltpu.VMEM(x.shape, bf16) for x in sources]
-        + [pltpu.SemaphoreType.DMA((4 + rings,))],
+        + [pltpu.SemaphoreType.DMA((6 + rings,))],
         name="pack",
         compiler_params=limit(4),
-    )(pinned(tokens.transpose(1, 0, 2)), *(pinned(x) for x in sources), turns)
+    )(*(pinned(x) for x in (tokens.transpose(1, 0, 2), *sources, *past)), turns)
     rows = lax.all_to_all(outgoing, "tp_0", split_axis=0, concat_axis=0, tiled=True)
     rows = lax.all_gather(rows, "tp_1", axis=0, tiled=True)
 
@@ -415,7 +427,7 @@
         + [pltpu.SemaphoreType.DMA((rings + 2,))],
         name="project",
         compiler_params=limit(12),
-    )(rows, turns, cached_latent_rows[0], past_rope[0].T, *(pinned(x) for x in sources))
+    )(rows, turns, *past, *(pinned(x) for x in sources))
     arrived = lax.all_to_all(lines, "sp", split_axis=0, concat_axis=0, tiled=True)
 
     count = prompts + EXTRA

time: 83.5 us -> 81.9 us (0.981)
  local copies, waits for them, and re-layouts: 2.55 us -> 0.03 us
  Pallas kernels: 7.67 us -> 8.52 us
    unnamed x12 -> x8, local copies, waits for them, and re-layouts: 2.55 us -> 0.03 us
    pallas_call x1, Pallas kernels: 1.27 us -> 2.12 us  [on_device(): pl.pallas_call(pack_kernel, out_shape=(shaped((rings, prompts + EXTRA + T...]
where the time goes in v2:
time: 81.9 us; the launch traced here: 81.6 us
  blocking collectives  72.2 us (88%)
  Pallas kernels  8.52 us (10%)
    all_to_all x1, blocking collectives, on_device(): lax.all_to_all(lines, 'sp', split_axis=0, concat_axis=0, tiled=True)  26.6 us
    all_to_all x1, blocking collectives, on_device(): lax.all_to_all(outgoing, 'tp_0', split_axis=0, concat_axis=0, tiled=True)  17.1 us
    all_to_all x1, blocking collectives, on_device(): got = lax.all_to_all(chunk, 'tp_0', split_axis=0, concat_axis=0, tiled=True)  14.1 us
    all_gather x1, blocking collectives, on_device(): rows = lax.all_gather(rows, 'tp_1', axis=0, tiled=True)  8.4 us
    all_gather x1, blocking collectives, on_device(): both = lax.all_gather(got, 'tp_1', axis=0, tiled=True)  5.94 us
    pallas_call x1, Pallas kernels, on_device(): pl.pallas_call(project_kernel, out_shape=(shaped((prompts, TILE, lanes)),...  3.28 us
    pallas_call x1, Pallas kernels, on_device(): pl.pallas_call(finish_kernel, out_shape=(shaped((row_count, key_up_weight...  2.94 us
    pallas_call x1, Pallas kernels, on_device(): pl.pallas_call(pack_kernel, out_shape=(shaped((rings, prompts + EXTRA + T...  2.12 us

profile of v2, /device:TPU:1, one launch (start us, length us, event | category | flops | bytes accessed | tf_op | source)
XLA Modules:
  0.0 81.6 jit_solution(8948002653490833030)
XLA Ops:
  0.7 0.1 fusion
  0.8 0.1 multiply_cosine_fusion
  0.9 2.1 %pack.1 = (bf16[8,72,256]{2,1,0:T(8,128)(2,1)S(1)}, f32[2,2,32]{2,1,0:T(2,128)S(1)}, bf16[2048,512]{1,0:T(8,128)(2,1)S(1)}, bf16[64,2048]{1,0:T(8,128)(2,1)S(1)}) custom-call(bf16[10,48,256]{2,1,0:T(8,128)(2,1)} %bitcast.17, bf16[1,256]{1,0:T(2,128)(2,1)} %nope_ref.1, bf16[1,128]{1,0:T(2,128)(2,1)} %turn_ref.1, bf16[512,256]{1,0:T(8,128)(2,1)} %key_ref.1, ...), custom_call_target="tpu_custom_call" | custom-call | tf_op jit(solution)/shard_map/pack/pallas_call | solution.py:397
  3.0 17.1 %all_to_all.15 = bf16[8,72,256]{2,1,0:T(8,128)(2,1)S(1)} all-to-all(bf16[8,72,256]{2,1,0:T(8,128)(2,1)S(1)} %get-tuple-element.15), channel_id=1, replica_groups=mesh['sp'=48,'tp_0'=8,'tp_1'=2] {'tp_0'}, dimensions={0} | all-to-all | bytes 589824 | tf_op jit(solution)/shard_map/all_to_all | solution.py:411
  20.1 8.4 %all_gather.6.rows_ref = bf16[16,72,256]{2,1,0:T(8,128)(2,1)S(1)} all-gather(bf16[8,72,256]{2,1,0:T(8,128)(2,1)S(1)} %all_to_all.15), channel_id=1, replica_groups=mesh['sp'=48,'tp_0'=8,'tp_1'=2] {'tp_1'}, dimensions={0}, use_global_device_ids=true | all-gather | bytes 884736 | tf_op jit(solution)/shard_map/all_gather | solution.py:412
  28.5 3.3 %project.1 = (bf16[48,8,128]{2,1,0:T(8,128)(2,1)S(1)}, bf16[8,8,512]{2,1,0:T(8,128)(2,1)S(1)}, f32[8,256]{1,0:T(8,128)S(1)}) custom-call(bf16[16,72,256]{2,1,0:T(8,128)(2,1)S(1)} %all_gather.6.rows_ref, f32[2,2,32]{2,1,0:T(2,128)S(1)} %get-tuple-element.16.angle_ref, bf16[2048,512]{1,0:T(8,128)(2,1)S(1)} %get-tuple-element.17.cached_ref, ...), custom_call_target="tpu_custom_call" | custom-call | tf_op jit(solution)/shard_map/project/pallas_call | solution.py:416
  31.8 0.0 copy-start
  31.8 0.0 copy-start.1
  31.8 0.0 copy-start.2
  31.8 0.0 copy-start.3
  31.9 26.6 %all_to_all.16.lines_ref = bf16[48,8,128]{2,1,0:T(8,128)(2,1)S(1)} all-to-all(bf16[48,8,128]{2,1,0:T(8,128)(2,1)S(1)} %get-tuple-element.19), channel_id=1, replica_groups=mesh['sp'=48,'tp_0'=8,'tp_1'=2] {'sp'}, dimensions={0} | all-to-all | bytes 196608 | tf_op jit(solution)/shard_map/all_to_all | solution.py:431
  58.5 0.2 chunk.1
  58.7 14.1 %all_to_all.17 = bf16[8,48,512]{2,1,0:T(8,128)(2,1)S(1)} all-to-all(bf16[8,48,512]{2,1,0:T(8,128)(2,1)S(1)} %chunk.1), channel_id=1, replica_groups=mesh['sp'=48,'tp_0'=8,'tp_1'=2] {'tp_0'}, dimensions={0} | all-to-all | bytes 786432 | tf_op jit(solution)/shard_map/all_to_all | solution.py:443
  72.7 5.9 %all_gather.7.both_ref = bf16[16,48,512]{2,1,0:T(8,128)(2,1)S(1)} all-gather(bf16[8,48,512]{2,1,0:T(8,128)(2,1)S(1)} %all_to_all.17), channel_id=1, replica_groups=mesh['sp'=48,'tp_0'=8,'tp_1'=2] {'tp_1'}, dimensions={0}, use_global_device_ids=true | all-gather | bytes 1179648 | tf_op jit(solution)/shard_map/all_gather | solution.py:444
  78.7 0.0 copy-done
  78.7 0.0 copy-done.1
  78.7 0.0 copy-done.2
  78.7 0.0 copy-done.3
  78.7 2.9 %finish.1 = (bf16[480,256]{1,0:T(8,128)(2,1)}, bf16[480,256]{1,0:T(8,128)(2,1)}, bf16[64,480]{1,0:T(8,128)(2,1)}, bf16[1,256]{1,0:T(2,128)(2,1)}) custom-call(bf16[16,48,512]{2,1,0:T(8,128)(2,1)S(1)} %all_gather.7.both_ref, bf16[512,256]{1,0:T(8,128)(2,1)S(1)} %copy-done, bf16[512,256]{1,0:T(8,128)(2,1)} %value_hbm.1, bf16[1,256]{1,0:T(2,128)(2,1)S(1)} %copy-done.2, ...), custom_call_target="tpu_custom_call" | custom-call | tf_op jit(solution)/shard_map/finish/pallas_call | solution.py:453
  (2 shorter events, 0.0 us)
Async XLA Ops:
  31.8 46.9 %copy-start = (bf16[512,256]{1,0:T(8,128)(2,1)S(1)}, bf16[512,256]{1,0:T(8,128)(2,1)}, u32[]{:S(2)}) copy-start(bf16[512,256]{1,0:T(8,128)(2,1)} %key_ref.1) | copy-start | bytes 786436
  31.8 46.9 %copy-start.1 = (s32[3,512]{1,0:T(4,128)S(1)}, s32[3,512]{1,0:T(4,128)}, u32[]{:S(2)}) copy-start(s32[3,512]{1,0:T(4,128)} %constant.40.clone.place_ref) | copy-start | bytes 18436
  31.8 46.9 %copy-start.2 = (bf16[1,256]{1,0:T(2,128)(2,1)S(1)}, bf16[1,256]{1,0:T(2,128)(2,1)}, u32[]{:S(2)}) copy-start(bf16[1,256]{1,0:T(2,128)(2,1)} %nope_ref.1) | copy-start | bytes 1540
  31.8 46.8 %copy-start.3 = (bf16[1,128]{1,0:T(2,128)(2,1)S(1)}, bf16[1,128]{1,0:T(2,128)(2,1)}, u32[]{:S(2)}) copy-start(bf16[1,128]{1,0:T(2,128)(2,1)} %turn_ref.1) | copy-start | bytes 772

commit v3 on v2

--- a/solution.py
+++ b/solution.py
@@ -179,9 +179,7 @@
 def read_cached(rows_ref, cached_ref, past_ref, sums_ref, stats_ref):
     ranks, count, features = rows_ref.shape
     rings = ranks // 2
-    width = cached_ref.shape[1]
     heads = 2 * ranks
-    group = heads // rings
     lines = rows_ref[:, count - TILE :, :].reshape(ranks * TILE, features)
     shape = (heads, ranks * TILE)
     head, line = iota(shape, 0), iota(shape, 1)
@@ -199,21 +197,12 @@
     weight = jnp.exp(score - peak)
     total = jnp.sum(weight, axis=-1, keepdims=True)
     summed = mm(weight.astype(bf16), cached)
-    high = summed.astype(bf16).astype(f32)
-    low = summed - high
-
-    shape = (heads, width // 2)
-    column = iota(shape, 1) // 8 - 6 * (iota(shape, 0) % group)
-    spread = jnp.zeros(shape, f32)
+    sums_ref[...] = summed
+    column = iota(stats_ref.shape, 1) - (stats_ref.shape[1] - ROPE // 2)
+    spread = jnp.zeros(stats_ref.shape, f32)
     for k, part in enumerate((*three(peak), *three(total))):
         spread = jnp.where(column == k, part, spread)
-    shape = (rings, heads)
-    wanted = jnp.where(iota(shape, 0) == iota(shape, 1) // group, 1.0, 0.0)
-    numbers = mm(wanted.astype(bf16), spread.astype(bf16))
-    for y in range(rings):
-        at = slice(group * y, group * (y + 1))
-        sums_ref[y] = jnp.concatenate([high[at], low[at]]).astype(bf16)
-    stats_ref[...] = numbers
+    stats_ref[...] = spread
 
 
 def chunk_kernel(lines_ref, sums_ref, stats_ref, out_ref, flat_ref):
@@ -244,36 +233,36 @@
     turned = jnp.concatenate(
         [turned[TILE * k : TILE * (k + 1)] for k in range(2 * count // TILE)], axis=1
     )
+    group = sums_ref.shape[0] // rings
     for y in range(rings):
+        at = slice(group * y, group * (y + 1))
+        sums = jnp.concatenate([sums_ref[at, : width // 2], sums_ref[at, width // 2 :]])
+        numbers = jnp.concatenate([jnp.zeros((group, lanes), f32), stats_ref[at, :]], axis=1)
+        numbers = jnp.concatenate([jnp.zeros((TILE - group, width // 2), f32), numbers])
         out_ref[y, :count, :] = latent
-        out_ref[y, count : count + TILE, :] = sums_ref[y]
-        numbers = jnp.concatenate(
-            [stats_ref[y : y + 1, :], jnp.zeros((TILE - 1, width // 2), f32)]
-        )
-        out_ref[y, count + TILE :, :] = jnp.concatenate([turned, numbers], axis=1).astype(bf16)
+        out_ref[y, count:, :] = jnp.concatenate([turned + numbers, sums], axis=1).astype(bf16)
 
 
 def finish_kernel(
     both_ref,
     key_ref,
-    value_hbm,
+    value_ref,
     nope_ref,
     turn_ref,
     place_ref,
-    keys_ref,
-    values_ref,
+    keys_hbm,
+    values_hbm,
     rope_ref,
     out_ref,
     latent_ref,
     turned_ref,
-    value_ref,
+    keys_ref,
+    values_ref,
     sem,
 ):
-    load = pltpu.make_async_copy(value_hbm, value_ref, sem)
-    load.start()
     sources, lines, width = both_ref.shape
     rings = sources // 2
-    count = lines - 2 * TILE
+    count = lines - TILE
     rows = keys_ref.shape[0]
     group = 4
     half = ROPE // 2
@@ -287,7 +276,7 @@
                 latent_ref[at, columns] = both_ref[
                     source, :count, upper * width // 2 : (upper + 1) * width // 2
                 ]
-            packed = both_ref[source, count + TILE :, :].astype(f32)
+            packed = both_ref[source, count:, :].astype(f32)
             halves.append(
                 jnp.concatenate(
                     [packed[:, half * k : half * (k + 1)] for k in range(2 * count // TILE)]
@@ -306,9 +295,12 @@
     turned = mm(move, turned_ref[...]).astype(bf16)
     keys = mm(latent, key_ref[...]).astype(bf16)
     keys_ref[...] = keys
-    load.wait()
+    stores = [pltpu.make_async_copy(keys_ref, keys_hbm, sem.at[0])]
+    stores[0].start()
     values = mm(latent, value_ref[...]).astype(bf16)
     values_ref[...] = values
+    stores.append(pltpu.make_async_copy(values_ref, values_hbm, sem.at[1]))
+    stores[1].start()
     same = jnp.where(iota((ROPE, ROPE), 0) == iota((ROPE, ROPE), 1), 1.0, 0.0).astype(bf16)
     rope = mm_nt(same, turned).astype(bf16)
     rope_ref[...] = rope
@@ -317,25 +309,25 @@
     turn = by_head(turn_ref[...], ROPE)
     score = (mm_nt(nope, keys) + mm(turn, jnp.concatenate([rope, rope], axis=0))) * FACTOR
 
-    shape = (group, width // 2)
-    place = iota(shape, 1) // 8 - 6 * iota(shape, 0)
-    mine = [(iota(shape, 1) % 8 == 0) & (place >= k) & (place < k + 3) for k in (0, 3)]
+    shape = (group, 2 * ROPE)
+    column = iota(shape, 1) - (2 * ROPE - half)
+    mine = [(column >= k) & (column < k + 3) for k in (0, 3)]
     peaks, totals = [], []
     for source in range(sources):
-        numbers = both_ref[source, count + TILE :, width // 2 :].astype(f32)[:1]
+        numbers = both_ref[source, count:, :].astype(f32)[group:, 2 * ROPE : 4 * ROPE]
         for found, where in zip((peaks, totals), mine):
             found.append(jnp.sum(jnp.where(where, numbers, 0.0), axis=-1, keepdims=True))
     past_peak = peaks[0]
     for x in peaks[1:]:
         past_peak = jnp.maximum(past_peak, x)
     past_total = jnp.zeros((group, 1), f32)
-    past_sum = jnp.zeros((TILE, width), f32)
+    past_sum = jnp.zeros((TILE, width // 2), f32)
     for k in range(sources):
         share = jnp.exp(peaks[k] - past_peak)
         past_total = past_total + totals[k] * share
-        sums = both_ref[k, count : count + TILE, :].astype(f32)
+        sums = both_ref[k, count:, width // 2 :].astype(f32)
         past_sum = past_sum + sums * jnp.concatenate([share, share])
-    past_sum = past_sum[:group] + past_sum[group:]
+    past_sum = jnp.concatenate([past_sum[:group], past_sum[group:]], axis=1)
 
     def own(x):
         half = group // 2
@@ -352,6 +344,8 @@
     shape = result.shape
     result = jnp.where(iota(shape, 1) // VALUE_WIDTH == iota(shape, 0), result, 0.0)
     out_ref[...] = jnp.sum(result, axis=0, keepdims=True).astype(bf16)
+    for store in stores:
+        store.wait()
 
 
 def shaped(shape, dtype=bf16):
@@ -412,13 +406,14 @@
     rows = lax.all_gather(rows, "tp_1", axis=0, tiled=True)
 
     lanes = 128
+    heads = 2 * lax.axis_size(TP)
     sources = (w_rope_key.T, latent_norm_gain[None], latent_down_weight)
     lines, sums, stats = pl.pallas_call(
         project_kernel,
         out_shape=(
             shaped((prompts, TILE, lanes)),
-            shaped((rings, TILE, width)),
-            shaped((rings, width // 2), f32),
+            shaped((heads, width), f32),
+            shaped((heads, lanes), f32),
         ),
         in_specs=[VMEM] * 4 + [HBM] * 3,
         out_specs=(VMEM,) * 3,
@@ -433,7 +428,7 @@
     count = prompts + EXTRA
     chunk = pl.pallas_call(
         chunk_kernel,
-        out_shape=shaped((rings, count // 2 + 2 * TILE, width)),
+        out_shape=shaped((rings, count // 2 + TILE, width)),
         in_specs=[VMEM] * 3,
         out_specs=VMEM,
         scratch_shapes=[pltpu.VMEM((prompts * TILE, lanes), f32)],
@@ -458,20 +453,21 @@
             shaped((ROPE, row_count)),
             shaped((1, value_up_weight.shape[1])),
         ),
-        in_specs=[VMEM, VMEM, HBM, VMEM, VMEM, VMEM],
-        out_specs=(VMEM,) * 4,
+        in_specs=[VMEM] * 6,
+        out_specs=(HBM, HBM, VMEM, VMEM),
         scratch_shapes=[
             pltpu.VMEM((rings * count, width), bf16),
             pltpu.VMEM((rings * count, ROPE), bf16),
-            pltpu.VMEM(value_up_weight.shape, bf16),
-            pltpu.SemaphoreType.DMA(()),
+            pltpu.VMEM((row_count, key_up_weight.shape[1]), bf16),
+            pltpu.VMEM((row_count, value_up_weight.shape[1]), bf16),
+            pltpu.SemaphoreType.DMA((2,)),
         ],
         name="finish",
         compiler_params=limit(8),
     )(
         both,
         key_up_weight,
-        pinned(value_up_weight),
+        value_up_weight,
         query_nope,
         query_rope,
         jnp.asarray(np.stack(tables), jnp.int32),

time: 81.9 us -> 81 us (0.989)
  blocking collectives: 72.2 us -> 70.6 us
    all_to_all x1, blocking collectives: 14.1 us -> 12.8 us  [on_device(): got = lax.all_to_all(chunk, 'tp_0', split_axis=0, concat_axis=0, tiled=True)]
    pallas_call x1, Pallas kernels: 3.28 us -> 4.11 us  [on_device(): pl.pallas_call(project_kernel, out_shape=(shaped((prompts, TILE, lanes)),...]
where the time goes in v3:
time: 81 us; the launch traced here: 80.7 us
  blocking collectives  70.6 us (87%)
  Pallas kernels  9.09 us (11%)
    all_to_all x1, blocking collectives, on_device(): lax.all_to_all(lines, 'sp', split_axis=0, concat_axis=0, tiled=True)  26.6 us
    all_to_all x1, blocking collectives, on_device(): lax.all_to_all(outgoing, 'tp_0', split_axis=0, concat_axis=0, tiled=True)  17.1 us
    all_to_all x1, blocking collectives, on_device(): got = lax.all_to_all(chunk, 'tp_0', split_axis=0, concat_axis=0, tiled=True)  12.8 us
    all_gather x1, blocking collectives, on_device(): rows = lax.all_gather(rows, 'tp_1', axis=0, tiled=True)  8.4 us
    all_gather x1, blocking collectives, on_device(): both = lax.all_gather(got, 'tp_1', axis=0, tiled=True)  5.66 us
    pallas_call x1, Pallas kernels, on_device(): pl.pallas_call(project_kernel, out_shape=(shaped((prompts, TILE, lanes)),...  4.11 us
    pallas_call x1, Pallas kernels, on_device(): pl.pallas_call(finish_kernel, out_shape=(shaped((row_count, key_up_weight...  2.67 us
    pallas_call x1, Pallas kernels, on_device(): pl.pallas_call(pack_kernel, out_shape=(shaped((rings, prompts + EXTRA + T...  2.12 us

profile of v3, /device:TPU:1, one launch (start us, length us, event | category | flops | bytes accessed | tf_op | source)
XLA Modules:
  0.0 80.7 jit_solution(8413021404055108293)
XLA Ops:
  0.7 0.1 fusion
  0.8 0.1 multiply_cosine_fusion
  0.9 2.1 %pack.1 = (bf16[8,72,256]{2,1,0:T(8,128)(2,1)S(1)}, f32[2,2,32]{2,1,0:T(2,128)S(1)}, bf16[2048,512]{1,0:T(8,128)(2,1)S(1)}, bf16[64,2048]{1,0:T(8,128)(2,1)S(1)}) custom-call(bf16[10,48,256]{2,1,0:T(8,128)(2,1)} %bitcast.17, bf16[1,256]{1,0:T(2,128)(2,1)} %nope_ref.1, bf16[1,128]{1,0:T(2,128)(2,1)} %turn_ref.1, bf16[512,256]{1,0:T(8,128)(2,1)} %key_ref.1, ...), custom_call_target="tpu_custom_call" | custom-call | tf_op jit(solution)/shard_map/pack/pallas_call | solution.py:391
  3.0 17.1 %all_to_all.15 = bf16[8,72,256]{2,1,0:T(8,128)(2,1)S(1)} all-to-all(bf16[8,72,256]{2,1,0:T(8,128)(2,1)S(1)} %get-tuple-element.15), channel_id=1, replica_groups=mesh['sp'=48,'tp_0'=8,'tp_1'=2] {'tp_0'}, dimensions={0} | all-to-all | bytes 589824 | tf_op jit(solution)/shard_map/all_to_all | solution.py:405
  20.1 8.4 %all_gather.6.rows_ref = bf16[16,72,256]{2,1,0:T(8,128)(2,1)S(1)} all-gather(bf16[8,72,256]{2,1,0:T(8,128)(2,1)S(1)} %all_to_all.15), channel_id=1, replica_groups=mesh['sp'=48,'tp_0'=8,'tp_1'=2] {'tp_1'}, dimensions={0}, use_global_device_ids=true | all-gather | bytes 884736 | tf_op jit(solution)/shard_map/all_gather | solution.py:406
  28.5 4.1 %project.1 = (bf16[48,8,128]{2,1,0:T(8,128)(2,1)S(1)}, f32[32,512]{1,0:T(8,128)S(1)}, f32[32,128]{1,0:T(8,128)S(1)}) custom-call(bf16[16,72,256]{2,1,0:T(8,128)(2,1)S(1)} %all_gather.6.rows_ref, f32[2,2,32]{2,1,0:T(2,128)S(1)} %get-tuple-element.16.angle_ref, bf16[2048,512]{1,0:T(8,128)(2,1)S(1)} %get-tuple-element.17.cached_ref, ...), custom_call_target="tpu_custom_call" | custom-call | tf_op jit(solution)/shard_map/project/pallas_call | solution.py:411
  32.6 0.0 copy-start
  32.7 0.0 copy-start.1
  32.7 0.0 copy-start.2
  32.7 0.0 copy-start.3
  32.7 0.0 copy-start.4
  32.7 26.6 %all_to_all.16.lines_ref = bf16[48,8,128]{2,1,0:T(8,128)(2,1)S(1)} all-to-all(bf16[48,8,128]{2,1,0:T(8,128)(2,1)S(1)} %get-tuple-element.19), channel_id=1, replica_groups=mesh['sp'=48,'tp_0'=8,'tp_1'=2] {'sp'}, dimensions={0} | all-to-all | bytes 196608 | tf_op jit(solution)/shard_map/all_to_all | solution.py:426
  59.3 0.2 chunk.1
  59.5 12.8 %all_to_all.17 = bf16[8,40,512]{2,1,0:T(8,128)(2,1)S(1)} all-to-all(bf16[8,40,512]{2,1,0:T(8,128)(2,1)S(1)} %chunk.1), channel_id=1, replica_groups=mesh['sp'=48,'tp_0'=8,'tp_1'=2] {'tp_0'}, dimensions={0} | all-to-all | bytes 655360 | tf_op jit(solution)/shard_map/all_to_all | solution.py:438
  72.4 5.7 %all_gather.7.both_ref = bf16[16,40,512]{2,1,0:T(8,128)(2,1)S(1)} all-gather(bf16[8,40,512]{2,1,0:T(8,128)(2,1)S(1)} %all_to_all.17), channel_id=1, replica_groups=mesh['sp'=48,'tp_0'=8,'tp_1'=2] {'tp_1'}, dimensions={0}, use_global_device_ids=true | all-gather | bytes 983040 | tf_op jit(solution)/shard_map/all_gather | solution.py:439
  78.0 0.0 copy-done
  78.0 0.0 copy-done.1
  78.0 0.0 copy-done.2
  78.0 0.0 copy-done.3
  78.0 0.0 copy-done.4
  78.0 2.7 %finish.1 = (bf16[480,256]{1,0:T(8,128)(2,1)}, bf16[480,256]{1,0:T(8,128)(2,1)}, bf16[64,480]{1,0:T(8,128)(2,1)}, bf16[1,256]{1,0:T(2,128)(2,1)}) custom-call(bf16[16,40,512]{2,1,0:T(8,128)(2,1)S(1)} %all_gather.7.both_ref, bf16[512,256]{1,0:T(8,128)(2,1)S(1)} %copy-done, bf16[512,256]{1,0:T(8,128)(2,1)S(1)} %copy-done.1, bf16[1,256]{1,0:T(2,128)(2,1)S(1)} %copy-done.3, ...), custom_call_target="tpu_custom_call" | custom-call | tf_op jit(solution)/shard_map/finish/pallas_call | solution.py:448
  (2 shorter events, 0.0 us)
Async XLA Ops:
  32.6 45.4 %copy-start = (bf16[512,256]{1,0:T(8,128)(2,1)S(1)}, bf16[512,256]{1,0:T(8,128)(2,1)}, u32[]{:S(2)}) copy-start(bf16[512,256]{1,0:T(8,128)(2,1)} %key_ref.1) | copy-start | bytes 786436
  32.7 45.4 %copy-start.1 = (bf16[512,256]{1,0:T(8,128)(2,1)S(1)}, bf16[512,256]{1,0:T(8,128)(2,1)}, u32[]{:S(2)}) copy-start(bf16[512,256]{1,0:T(8,128)(2,1)} %value_ref.1) | copy-start | bytes 786436
  32.7 45.4 %copy-start.2 = (s32[3,512]{1,0:T(4,128)S(1)}, s32[3,512]{1,0:T(4,128)}, u32[]{:S(2)}) copy-start(s32[3,512]{1,0:T(4,128)} %constant.40.clone.place_ref) | copy-start | bytes 18436
  32.7 45.3 %copy-start.3 = (bf16[1,256]{1,0:T(2,128)(2,1)S(1)}, bf16[1,256]{1,0:T(2,128)(2,1)}, u32[]{:S(2)}) copy-start(bf16[1,256]{1,0:T(2,128)(2,1)} %nope_ref.1) | copy-start | bytes 1540
  32.7 45.3 %copy-start.4 = (bf16[1,128]{1,0:T(2,128)(2,1)S(1)}, bf16[1,128]{1,0:T(2,128)(2,1)}, u32[]{:S(2)}) copy-start(bf16[1,128]{1,0:T(2,128)(2,1)} %turn_ref.1) | copy-start | bytes 772
